TPU v7x, 32 devices: a whole 2x2x4 slice. The times are simulated.
32 devices in a mesh: sp: 8 (over z, x), tp: 4 (over y, core).
Axes of the slice: x: 2, y: 2, z: 4, core: 2. Of those that a mesh axis runs over, the one named last changes fastest.
Arguments:
- queries: bfloat16 [3072, 1024], P('sp', 'tp'), may hold values from -160 to 160
- key_vectors: bfloat16 [3072, 1024], P('sp', 'tp'), may hold values from -7 to 7
- values: bfloat16 [3072, 1024], P('sp', 'tp'), may hold values from -6 to 6
- head_lambda: float32 [8], P('tp'), may hold values from 0.3 to 0.8
- head_gain: float32 [128], replicated, may hold values from 0.1 to 1.9
- w_out: bfloat16 [1024, 2048], P('tp'), may hold values from -0.1875 to 0.1875
- residual: bfloat16 [3072, 2048], P(('sp', 'tp')), may hold values from -6 to 6
- ffn_gain: float32 [2048], replicated, may hold values from 0.1 to 1.9
- route_ids: int32 [3072, 2], P(('sp', 'tp')), may hold values from 0 to 7, all different within a row; in each aligned block of 96 rows (0 to 95, 96 to 191, ...) at most 30 rows name the same one
- route_logits: float32 [3072, 2], P(('sp', 'tp')), may hold values from -8 to 310
- w_gate: bfloat16 [8, 2048, 2048], P('sp', None, 'tp'), may hold values from -0.3125 to 0.3125
- w_up: bfloat16 [8, 2048, 2048], P('sp', None, 'tp'), may hold values from -0.3125 to 0.3125
- w_down: bfloat16 [8, 2048, 2048], P('sp', 'tp'), may hold values from -0.125 to 0.125
Outputs:
- layer_out: bfloat16 [3072, 2048], P(('sp', 'tp'))
Inputs may be any that keep to these rules, and one draw needn't show every extreme that they name: `route_ids`: in the rows of one device after the attention (aligned blocks of 96 rows) no expert is named by more than 30 rows, a bound that some block reaches while other experts in the same block get fewer rows; each row names 2 different experts.
All inputs are finite; a program needn't handle non-finite values.
Results may differ from a plain program's by a relative error of at most 0.023.
Values may be sent and summed in bfloat16 or wider, within the bound.
A program may use at most 192 MiB of HBM per device.

v0:
```python
import jax
import jax.numpy as jnp
from jax import lax
from jax.sharding import PartitionSpec as P

SEGMENT = 64
SEQUENCES = 1


EPS = 1e-06
NEG = -1e30
CLAMP = 7.0
ALPHA = 1.702
OUT_FACTOR = 0.8


def shards(
    queries,
    key_vectors,
    values,
    head_lambda,
    head_gain,
    w_out,
    residual,
    ffn_gain,
    route_ids,
    route_logits,
    w_gate,
    w_up,
    w_down,
):
    tok_count = queries.shape[0]
    local_heads = head_lambda.shape[0]
    head_width = queries.shape[1] // (2 * local_heads)
    value_width = values.shape[1] // local_heads
    score_scale = head_width ** (-0.5)
    n_tp = lax.axis_size("tp")
    n_sp = lax.axis_size("sp")
    seq_length = tok_count * n_sp // SEQUENCES
    query_pos = lax.axis_index("sp") * tok_count + jnp.arange(tok_count, dtype=jnp.int32)
    query_seg = query_pos // SEGMENT
    query_seq = query_pos // seq_length
    seq_begin = query_seq[0] * seq_length
    last_seg = query_seg[tok_count - 1]
    query_heads = queries.reshape(tok_count, local_heads, 2, head_width)

    def absorb(carry, key_block, value_block, key_start):
        maxima, totals, sums = carry
        block_len = key_block.shape[0]
        key_pos = key_start + jnp.arange(block_len, dtype=jnp.int32)
        visible = ((key_pos // SEGMENT)[None, :] <= query_seg[:, None]) & (
            (key_pos // seq_length)[None, :] == query_seq[:, None]
        )
        score = (
            jnp.einsum(
                "qhjd,khjd->jhqk", query_heads, key_block, preferred_element_type=jnp.float32
            )
            * score_scale
        )
        score = jnp.where(visible, score, NEG)
        new_max = jnp.maximum(maxima, jnp.max(score, axis=-1))
        expo = jnp.where(visible, jnp.exp(score - new_max[..., None]), 0.0)
        factor = jnp.exp(maxima - new_max)
        totals = totals * factor + jnp.sum(expo, axis=-1)
        added = jnp.einsum(
            "jhqk,khd->jqhd",
            expo.astype(jnp.bfloat16),
            value_block,
            preferred_element_type=jnp.float32,
        )
        sums = sums * jnp.transpose(factor, (0, 2, 1))[..., None] + added
        return (new_max, totals, sums)

    def maybe_absorb(carry, key_block, value_block, key_start):
        block_len = key_block.shape[0]
        needed = (key_start // SEGMENT <= last_seg) & (key_start + block_len - 1 >= seq_begin)
        return lax.cond(
            needed,
            lambda inner: absorb(inner, key_block, value_block, key_start),
            lambda inner: inner,
            carry,
        )

    initial = (
        jnp.full((2, local_heads, tok_count), NEG, jnp.float32),
        jnp.zeros((2, local_heads, tok_count), jnp.float32),
        jnp.zeros((2, tok_count, local_heads, value_width), jnp.float32),
    )
    key_piece = lax.all_gather(key_vectors, "sp", axis=0, tiled=True)
    value_piece = lax.all_gather(values, "sp", axis=0, tiled=True)
    piece_len = key_piece.shape[0]
    key_rows = key_piece.reshape(piece_len, local_heads, 2, head_width)
    value_rows = value_piece.reshape(piece_len, local_heads, value_width)
    key_step = 512

    def advance(block_index, inner):
        key_offset = block_index * key_step
        key_block = lax.dynamic_slice_in_dim(key_rows, key_offset, key_step, 0)
        value_block = lax.dynamic_slice_in_dim(value_rows, key_offset, key_step, 0)
        return maybe_absorb(inner, key_block, value_block, key_offset)

    maxima, totals, sums = lax.fori_loop(0, piece_len // key_step, advance, initial)
    attended = sums / jnp.transpose(totals, (0, 2, 1))[..., None]
    diff = attended[0] - head_lambda[None, :, None] * attended[1]
    scale_rows = lax.rsqrt(jnp.mean(diff * diff, axis=-1, keepdims=True) + EPS)
    head_rows = (diff * scale_rows * head_gain * OUT_FACTOR).astype(jnp.bfloat16)
    head_rows = head_rows.reshape(tok_count, local_heads * value_width)
    own_count = tok_count // n_tp
    whole_weight = lax.all_gather(w_out, "tp", axis=0, tiled=True)
    token_heads = lax.all_to_all(head_rows, "tp", split_axis=0, concat_axis=1, tiled=True)
    projected = jnp.dot(token_heads, whole_weight, preferred_element_type=jnp.float32)
    mixed = (residual.astype(jnp.float32) + projected).astype(jnp.bfloat16)
    mixed32 = mixed.astype(jnp.float32)
    normed = (
        mixed32 * lax.rsqrt(jnp.mean(mixed32 * mixed32, axis=-1, keepdims=True) + EPS) * ffn_gain
    ).astype(jnp.bfloat16)
    gates = jax.nn.softmax(route_logits, axis=-1)
    top_count = route_ids.shape[1]
    model_width = normed.shape[1]
    cap_slots = max(2, 5 * top_count * tok_count // (4 * n_tp * n_sp))
    flat_ids = route_ids.reshape(-1)
    chosen = (flat_ids[:, None] == jnp.arange(n_sp, dtype=jnp.int32)[None, :]).astype(jnp.int32)
    earlier = jnp.cumsum(chosen, axis=0) - chosen
    slot_rank = jnp.sum(earlier * chosen, axis=1)
    slot_index = flat_ids * cap_slots + slot_rank
    source_rows = jnp.repeat(normed, top_count, axis=0)
    outgoing = (
        jnp.zeros((n_sp * cap_slots, model_width), jnp.bfloat16).at[slot_index].set(source_rows)
    )
    outgoing = outgoing.reshape(n_sp, cap_slots, model_width)
    arrived = lax.all_to_all(outgoing, "sp", split_axis=0, concat_axis=0, tiled=True)
    senders, slot_count, arrived_width = arrived.shape
    flat_in = arrived.reshape(senders * slot_count, arrived_width)
    piece = lax.all_gather(flat_in, "tp", axis=0, tiled=True)
    gate_pre = jnp.dot(piece, w_gate[0], preferred_element_type=jnp.float32)
    up_pre = jnp.dot(piece, w_up[0], preferred_element_type=jnp.float32)
    gate_cut = jnp.minimum(gate_pre, CLAMP)
    up_cut = jnp.clip(up_pre, -CLAMP, CLAMP)
    active = (gate_cut * jax.nn.sigmoid(ALPHA * gate_cut) * (up_cut + 1.0)).astype(jnp.bfloat16)
    reduced = lax.psum_scatter(
        jnp.dot(active, w_down[0], preferred_element_type=jnp.float32).astype(jnp.bfloat16),
        "tp",
        scatter_dimension=0,
        tiled=True,
    )
    reduced = reduced.reshape(senders, slot_count, arrived_width)
    returned = lax.all_to_all(reduced, "sp", split_axis=0, concat_axis=0, tiled=True)
    picked = returned.reshape(n_sp * cap_slots, model_width)[slot_index].astype(jnp.float32)
    weighted = (picked * gates.reshape(-1)[:, None]).reshape(own_count, top_count, model_width)
    return (mixed32 + jnp.sum(weighted, axis=1)).astype(jnp.bfloat16)


def solution(mesh):
    in_specs = (
        P("sp", "tp"),
        P("sp", "tp"),
        P("sp", "tp"),
        P("tp"),
        P(),
        P("tp", None),
        P(("sp", "tp"), None),
        P(),
        P(("sp", "tp"), None),
        P(("sp", "tp"), None),
        P("sp", None, "tp"),
        P("sp", None, "tp"),
        P("sp", "tp", None),
    )
    out_specs = P(("sp", "tp"), None)
    return jax.shard_map(shards, mesh=mesh, in_specs=in_specs, out_specs=out_specs, check_vma=False)
```

profile of v0, /device:TPU:13, one launch (start us, length us, event | category | flops | bytes accessed | tf_op | source)
XLA Modules:
  0.0 333.0 jit_solution(3574506045380296739)
XLA Ops:
  6.6 1.9 copy.37
  8.6 1.8 copy.39
  14.6 37.9 %all-gather.5.cloned.1.call-done = bf16[3072,256]{0,1:T(8,128)(2,1)} async-done(((bf16[384,256]{0,1:T(8,128)(2,1)}), bf16[3072,256]{0,1:T(8,128)(2,1)}) %all-gather.5.cloned.1.call-update) | async-done | bytes 1572880 | tf_op jit(solution)/shard_map/all_gather | solution.py:89
  52.6 2.7 copy.40
  55.3 42.0 %all-gather.7.cloned.1.call-done = bf16[3072,256]{0,1:T(8,128)(2,1)} async-done(((bf16[384,256]{0,1:T(8,128)(2,1)}), bf16[3072,256]{0,1:T(8,128)(2,1)}) %all-gather.7.cloned.1.call-update) | async-done | bytes 1572880 | tf_op jit(solution)/shard_map/all_gather | solution.py:90
  97.3 2.6 copy.42
  99.9 19.3 %while.24 = (s32[]{:T(128)}, f32[2,2,384]{2,1,0:T(2,128)S(1)}, f32[2,2,384]{2,1,0:T(2,128)S(1)}, f32[2,384,2,128]{3,1,0,2:T(8,128)S(1)}, s32[]{:T(128)}, /*index...) while((s32[]{:T(128)}, f32[2,2,384]{2,1,0:T(2,128)S(1)}, ...), condition=%wide.region_5.6_spmd.clone.clone, body=%wide.region_0.5_spmd.clone.clone.sunk | while | flops 310077472 | bytes 12468234 | solution.py:102
  100.7 4.9 %conditional.4 = ((f32[2,2,384]{2,1,0:T(2,128)S(1)}, f32[2,2,384]{2,1,0:T(2,128)S(1)}, f32[2,384,2,128]{3,1,0,2:T(8,128)S(1)})) conditional(s32[]{:T(128)} %convert_element_type.87, (f32[2,2,384]{2,1,0:T(2,128)S(1)}, f32[2,2,384]{2,1,0:T(2,128)S(1)}, f32[2,384,2,128]{3,1,0,2:T(8,128)S(1)}) %tuple.101, (s32[]{:T(128)}, ...), branch_computations={%region_1.1_spmd, %region_2.4_spmd.clone} | conditional | flops 310070912 | bytes 12456133 | solution.py:77
  101.1 1.7 fusion.4
  103.7 1.9 fusion.12
  106.3 5.0 %conditional.4 = ((f32[2,2,384]{2,1,0:T(2,128)S(1)}, f32[2,2,384]{2,1,0:T(2,128)S(1)}, f32[2,384,2,128]{3,1,0,2:T(8,128)S(1)})) conditional(s32[]{:T(128)} %convert_element_type.87, (f32[2,2,384]{2,1,0:T(2,128)S(1)}, f32[2,2,384]{2,1,0:T(2,128)S(1)}, f32[2,384,2,128]{3,1,0,2:T(8,128)S(1)}) %tuple.101, (s32[]{:T(128)}, ...), branch_computations={%region_1.1_spmd, %region_2.4_spmd.clone} | conditional | flops 310070912 | bytes 12456133 | solution.py:77
  106.7 1.7 fusion.4
  109.4 1.9 fusion.12
  112.0 4.9 %conditional.4 = ((f32[2,2,384]{2,1,0:T(2,128)S(1)}, f32[2,2,384]{2,1,0:T(2,128)S(1)}, f32[2,384,2,128]{3,1,0,2:T(8,128)S(1)})) conditional(s32[]{:T(128)} %convert_element_type.87, (f32[2,2,384]{2,1,0:T(2,128)S(1)}, f32[2,2,384]{2,1,0:T(2,128)S(1)}, f32[2,384,2,128]{3,1,0,2:T(8,128)S(1)}) %tuple.101, (s32[]{:T(128)}, ...), branch_computations={%region_1.1_spmd, %region_2.4_spmd.clone} | conditional | flops 310070912 | bytes 12456133 | solution.py:77
  115.0 1.9 fusion.12
  126.2 1.8 multiply_convert_fusion.2
  127.9 5.5 %all-to-all-start = ((bf16[4,96,256]{2,1,0:T(8,128)(2,1)}), bf16[4,96,256]{2,1,0:T(8,128)(2,1)S(1)}, u32[]{:S(2)}, u32[]{:S(2)}) async-start(bf16[4,96,256]{2,1,0:T(8,128)(2,1)} %multiply_convert_fusion.2), calls=%async_computation | async-start | bytes 393216 | tf_op jit(solution)/shard_map/all_to_all | solution.py:110
  133.4 3.5 %all-to-all-done = bf16[4,96,256]{2,1,0:T(8,128)(2,1)S(1)} async-done(((bf16[4,96,256]{2,1,0:T(8,128)(2,1)}), bf16[4,96,256]{2,1,0:T(8,128)(2,1)S(1)}, u32[]{:S(2)}, u32[]{:S(2)}) %all-to-all-start) | async-done | bytes 196640 | tf_op jit(solution)/shard_map/all_to_all | solution.py:110
  136.9 3.2 multiply_reduce_fusion.1
  142.9 3.3 %scatter_custom_fusion = bf16[240,2048]{1,0:T(8,128)(2,1)} fusion(s32[192]{0:T(256)S(1)} %bitcast.84, bf16[192,2048]{1,0:T(8,128)(2,1)} %reshape.176, bf16[]{:T(256)} %constant.234.clone.1), kind=kCustom, calls=%fused_computation.63 | custom fusion | bytes 983552 | tf_op jit(solution)/shard_map/scatter | solution.py:128
  147.7 42.3 %all_to_all.26 = bf16[8,30,2048]{2,1,0:T(8,128)(2,1)} all-to-all(bf16[8,30,2048]{2,1,0:T(8,128)(2,1)S(1)} %reshape.158), channel_id=1, replica_groups=mesh['sp'=8,'tp'=4] {'sp'}, dimensions={0} | all-to-all | bytes 1966080 | tf_op jit(solution)/shard_map/all_to_all | solution.py:131
  190.0 2.4 reshape.159
  192.7 33.2 %all-gather.11.cloned.1.call-done = bf16[960,2048]{1,0:T(8,128)(2,1)} async-done(((bf16[240,2048]{1,0:T(8,128)(2,1)}), bf16[960,2048]{1,0:T(8,128)(2,1)}) %all-gather.11.cloned.1.call-update) | async-done | bytes 3932176 | tf_op jit(solution)/shard_map/all_gather | solution.py:134
  225.9 6.3 %fusion.35 = f32[960,512]{1,0:T(8,128)} fusion(bf16[960,2048]{1,0:T(8,128)(2,1)} %all-gather.11.cloned.1.call-done, bf16[1,2048,512]{2,1,0:T(8,128)(2,1)} %param.28), kind=kOutput, calls=%fused_computation.54 | convolution fusion | flops 2013265920 | bytes 7995392 | tf_op jit(solution)/shard_map/dot_general | solution.py:136
  232.2 9.8 %convolution_convert_fusion = bf16[960,2048]{1,0:T(8,128)(2,1)} fusion(bf16[1,512,2048]{2,1,0:T(8,128)(2,1)S(1)} %copy-done, f32[960,512]{1,0:T(8,128)} %fusion.35, bf16[960,2048]{1,0:T(8,128)(2,1)} %all-gather.11.cloned.1.call-done, bf16[1,2048,512]{2,1,0:T(8,128)(2,1)} %param.27), kind=kOutput, calls=%fused_computation.49 | convolution fusion | flops 4033413120 | bytes 14024704 | tf_op jit(solution)/shard_map/dot_general | solution.py:141
  242.1 42.5 %reduce-scatter.2.cloned.1.call-done = bf16[240,2048]{1,0:T(8,128)(2,1)} async-done(((bf16[960,2048]{1,0:T(8,128)(2,1)}), bf16[240,2048]{1,0:T(8,128)(2,1)}) %reduce-scatter.2.cloned.1.call-update) | async-done | bytes 983056 | tf_op jit(solution)/shard_map/reduce_scatter | solution.py:140
  284.6 2.4 reshape.160
  287.0 5.5 %all-to-all-start.2 = ((bf16[8,30,2048]{2,1,0:T(8,128)(2,1)}), bf16[8,30,2048]{2,1,0:T(8,128)(2,1)}, u32[]{:S(2)}, u32[]{:S(2)}) async-start(bf16[8,30,2048]{2,1,0:T(8,128)(2,1)} %reshape.160), calls=%async_computation.3 | async-start | bytes 2097152 | tf_op jit(solution)/shard_map/all_to_all | solution.py:147
  292.7 22.7 %all-to-all-done.2 = bf16[8,30,2048]{2,1,0:T(8,128)(2,1)} async-done(((bf16[8,30,2048]{2,1,0:T(8,128)(2,1)}), bf16[8,30,2048]{2,1,0:T(8,128)(2,1)}, u32[]{:S(2)}, u32[]{:S(2)}) %all-to-all-start.2) | async-done | bytes 983072 | tf_op jit(solution)/shard_map/all_to_all | solution.py:147
  316.8 2.0 gather_fusion
  318.9 3.0 reshape.163
  321.9 3.7 %multiply_reduce_fusion = f32[96,2048]{1,0:T(8,128)S(1)} fusion(f32[96,2,2048]{2,1,0:T(2,128)} %reshape.163, f32[96,2]{1,0:T(8,128)S(1)} %copy.51), kind=kLoop, calls=%fused_computation.59 | loop fusion | flops 589824 | bytes 2360064 | tf_op jit(solution)/shard_map/reduce_sum | solution.py:150
  (147 shorter events, 23.4 us)
Async XLA Ops:
  6.5 225.7 %copy-start = (bf16[1,512,2048]{2,1,0:T(8,128)(2,1)S(1)}, bf16[1,512,2048]{2,1,0:T(8,128)(2,1)}, u32[]{:S(2)}) copy-start(bf16[1,512,2048]{2,1,0:T(8,128)(2,1)} %param.29) | copy-start | bytes 6291460
  6.5 5.7 %copy-start.6 = (bf16[384,256]{1,0:T(8,128)(2,1)S(1)}, bf16[384,256]{1,0:T(8,128)(2,1)}, u32[]{:S(2)}) copy-start(bf16[384,256]{1,0:T(8,128)(2,1)} %param.17) | copy-start | bytes 589828
  6.5 5.9 %copy-start.9 = (s32[96,2]{0,1:T(2,128)S(1)}, s32[96,2]{0,1:T(2,128)}, u32[]{:S(2)}) copy-start(s32[96,2]{0,1:T(2,128)} %param.25) | copy-start | bytes 2308
  6.5 8.0 %copy-start.10 = (f32[2]{0:T(128)S(1)}, f32[2]{0:T(128)}, u32[]{:S(2)}) copy-start(f32[2]{0:T(128)} %param.20) | copy-start | bytes 28
  6.5 8.0 %copy-start.11 = (f32[128]{0:T(128)S(1)}, f32[128]{0:T(128)}, u32[]{:S(2)}) copy-start(f32[128]{0:T(128)} %param.21) | copy-start | bytes 1540
  6.5 46.0 %all-gather.5.cloned.1.call-start = ((), (), s32[]{:S(2)}) async-start(), calls=%async_computation.4 | async-start | bytes 1769472 | tf_op jit(solution)/shard_map/all_gather | solution.py:89
  8.5 88.8 %all-gather.7.cloned.1.call-start = ((), (), s32[]{:S(2)}) async-start(), calls=%async_computation.5 | async-start | bytes 1769472 | tf_op jit(solution)/shard_map/all_gather | solution.py:90
  10.3 126.6 %all-gather.9.cloned.1.call-start = ((), (), s32[]{:S(2)}) async-start(), calls=%async_computation.6 | async-start | bytes 5242880 | tf_op jit(solution)/shard_map/all_gather | solution.py:109
  119.5 0.9 copy-start.1
  121.2 3.8 %copy-start.2 = (f32[2,384,2,128]{3,1,0,2:T(8,128)S(1)}, f32[2,384,2,128]{3,1,0,2:T(8,128)}, u32[]{:S(2)}) copy-start(f32[2,384,2,128]{3,1,0,2:T(8,128)} %copy-done.1) | copy-start | bytes 2359300
  124.9 1.2 copy-start.5
  127.9 9.0 %all-to-all-start = ((bf16[4,96,256]{2,1,0:T(8,128)(2,1)}), bf16[4,96,256]{2,1,0:T(8,128)(2,1)S(1)}, u32[]{:S(2)}, u32[]{:S(2)}) async-start(bf16[4,96,256]{2,1,0:T(8,128)(2,1)} %multiply_convert_fusion.2), calls=%async_computation | async-start | bytes 393216 | tf_op jit(solution)/shard_map/all_to_all | solution.py:110
  133.4 92.5 %all-gather.11.cloned.1.call-start = ((), (), s32[]{:S(2)}) async-start(), calls=%async_computation.7 | async-start | bytes 4915200 | tf_op jit(solution)/shard_map/all_gather | solution.py:134
  136.9 4.1 %copy-start.8 = (f32[2048]{0:T(1024)S(1)}, f32[2048]{0:T(1024)}, u32[]{:S(2)}) copy-start(f32[2048]{0:T(1024)} %param.24) | copy-start | bytes 24580
  140.2 0.9 copy-start.3
  192.5 92.1 %reduce-scatter.2.cloned.1.call-start = ((), (), s32[]{:S(2)}) async-start(), calls=%async_computation.8 | async-start | bytes 4915200 | tf_op jit(solution)/shard_map/reduce_scatter | solution.py:140
  242.1 50.4 %copy-start.7 = (f32[96,2]{0,1:T(2,128)S(1)}, f32[96,2]{0,1:T(2,128)}, u32[]{:S(2)}) copy-start(f32[96,2]{0,1:T(2,128)} %param.26) | copy-start | bytes 2308
  287.0 28.3 %all-to-all-start.2 = ((bf16[8,30,2048]{2,1,0:T(8,128)(2,1)}), bf16[8,30,2048]{2,1,0:T(8,128)(2,1)}, u32[]{:S(2)}, u32[]{:S(2)}) async-start(bf16[8,30,2048]{2,1,0:T(8,128)(2,1)} %reshape.160), calls=%async_computation.3 | async-start | bytes 2097152 | tf_op jit(solution)/shard_map/all_to_all | solution.py:147
  318.9 6.8 %copy-start.4 = (f32[96,2048]{1,0:T(8,128)S(1)}, f32[96,2048]{1,0:T(8,128)}, u32[]{:S(2)}) copy-start(f32[96,2048]{1,0:T(8,128)} %copy-done.3) | copy-start | bytes 2359300
Sparse Core Ops, SparseCore 0:
  9.4 43.1 all-gather.4
  54.6 42.5 all-gather.6
  98.8 34.5 all-gather.8
  192.6 33.2 all-gather.10
  242.2 42.3 reduce-scatter.1
where the time goes:
time: 340 us; the launch traced here: 333 us
  waiting for transfers between devices  183 us (54%)
  blocking collectives  42.3 us (12%)
  local copies, waits for them, and re-layouts  36.4 us (11%)
  matrix products  30 us (9%)
  between operations  14 us (4%)
  other arithmetic  11.8 us (3%)
  starting transfers between devices  11.3 us (3%)
  loops' own time  4.54 us (1%)
    reduce_scatter x1, waiting for transfers between devices, shards(): lax.psum_scatter(jnp.dot(active, w_down[0], preferred_element_type=jnp.fl...  42.5 us
    all_to_all x1, blocking collectives, shards(): lax.all_to_all(outgoing, 'sp', split_axis=0, concat_axis=0, tiled=True)  42.3 us
    all_gather x1, waiting for transfers between devices, shards(): value_piece = lax.all_gather(values, 'sp', axis=0, tiled=True)  42 us
    all_gather x1, waiting for transfers between devices, shards(): key_piece = lax.all_gather(key_vectors, 'sp', axis=0, tiled=True)  37.9 us
    all_gather x1, waiting for transfers between devices, shards(): piece = lax.all_gather(flat_in, 'tp', axis=0, tiled=True)  33.2 us
    all_to_all x1, waiting for transfers between devices, shards(): lax.all_to_all(reduced, 'sp', split_axis=0, concat_axis=0, tiled=True)  22.7 us
    unnamed x31, local copies, waits for them, and re-layouts  11 us
    dot_general x1, matrix products, shards(): jnp.dot(active, w_down[0], preferred_element_type=jnp.float32)  9.82 us
  transfers between devices with their start and end apart: 7, of which 6 were waited for; matrix products, arithmetic and copies ran while one was open for 10% of the time, Pallas kernels for 0%

commit v1 on v0

v1 whole, which is shorter than its diff:
```python
import functools

import jax
import jax.numpy as jnp
from jax import lax
from jax.experimental import pallas as pl
from jax.experimental.pallas import tpu as pltpu
from jax.sharding import PartitionSpec as P

SEGMENT = 64
EPS = 1e-06
NEG = -1e30
CLAMP = 7.0
ALPHA = 1.702
OUT_FACTOR = 0.8

MESH = pl.DeviceIdType.MESH
F32 = jnp.float32
BF16 = jnp.bfloat16
VMEM = pl.BlockSpec(memory_space=pltpu.VMEM)
SMEM = pl.BlockSpec(memory_space=pltpu.SMEM)


def remote(src, dst, send_sem, recv_sem, axis, index):
    return pltpu.make_async_remote_copy(
        src_ref=src,
        dst_ref=dst,
        send_sem=send_sem,
        recv_sem=recv_sem,
        device_id={axis: index},
        device_id_type=MESH,
    )


def greet(axis, index):
    barrier = pltpu.get_barrier_semaphore()
    pl.semaphore_signal(barrier, inc=1, device_id={axis: index}, device_id_type=MESH)


def attend_kernel(
    dims, lam_ref, qt_ref, k_ref, vt_ref, gain_ref, out_ref,
    kbuf, vbuf, acc, top, tot, rows_ref, col_send, pair_send, recv, tp_send, tp_recv,
):
    n_sp, n_tp, heads, width, vwidth, toks = dims
    me = lax.axis_index("sp")
    t = lax.axis_index("tp")
    z, x = me // 2, me % 2
    levels = n_sp // 2
    pair = 2 * z + 1 - x
    barrier = pltpu.get_barrier_semaphore()
    greet("sp", pair)
    for d in range(1, n_tp):
        greet("tp", (t + d) % n_tp)

    @pl.when(z > 0)
    def _():
        greet("sp", jnp.maximum(me - 2, 0))

    @pl.when(z < levels - 1)
    def _():
        greet("sp", jnp.minimum(me + 2, n_sp - 1))

    beside = jnp.minimum(z, 1) + jnp.minimum(levels - 1 - z, 1)
    pl.semaphore_wait(barrier, n_tp + beside)
    below = jnp.minimum(me + 2, n_sp - 1)

    def copies(block, k_src, v_src, sems, axis_target):
        return (
            remote(k_src, kbuf.at[block], sems.at[0, block], recv.at[0, block], "sp", axis_target),
            remote(v_src, vbuf.at[block], sems.at[1, block], recv.at[1, block], "sp", axis_target),
        )

    def start(parts):
        for part in parts:
            part.start()

    @pl.when(z < levels - 1)
    def _():
        start(copies(me, k_ref, vt_ref, col_send, below))

    @pl.when(x == 0)
    def _():
        start(copies(me, k_ref, vt_ref, pair_send, pair))

    def absorb(kb, vb, first):
        if first:
            shape = (toks, toks)
            kseg = lax.broadcasted_iota(jnp.int32, shape, 0) // SEGMENT
            qseg = lax.broadcasted_iota(jnp.int32, shape, 1) // SEGMENT
            visible = kseg <= qseg
        for h in range(heads):
            for j in range(2):
                i = 2 * h + j
                keys = kb[:, i * width:(i + 1) * width]
                qs = qt_ref[i * width:(i + 1) * width, :]
                score = jnp.dot(keys, qs, preferred_element_type=F32)
                if first:
                    score = jnp.where(visible, score, NEG)
                high = jnp.max(score, axis=0, keepdims=True)
                if not first:
                    old = top[i:i + 1, :]
                    high = jnp.maximum(high, old)
                expo = jnp.exp(score - high)
                if first:
                    expo = jnp.where(visible, expo, 0.0)
                total = jnp.sum(expo, axis=0, keepdims=True)
                added = jnp.dot(
                    vb[h * vwidth:(h + 1) * vwidth, :], expo.astype(BF16),
                    preferred_element_type=F32,
                )
                if first:
                    acc[i] = added
                else:
                    factor = jnp.exp(old - high)
                    total = total + tot[i:i + 1, :] * factor
                    acc[i] = acc[i] * factor + added
                top[i:i + 1, :] = high
                tot[i:i + 1, :] = total

    absorb(k_ref, vt_ref, True)

    def arrive(block):
        for part in copies(block, k_ref, vt_ref, col_send, me):
            part.wait_recv()

    @pl.when(x == 1)
    def _():
        arrive(pair)
        absorb(kbuf.at[pair], vbuf.at[pair], False)

    def level(c, carry):
        block = me - 2 * (c + 1)
        arrive(block)

        @pl.when(z < levels - 1)
        def _():
            start(copies(block, kbuf.at[block], vbuf.at[block], col_send, below))

        start(copies(block, kbuf.at[block], vbuf.at[block], pair_send, pair))
        absorb(kbuf.at[block], vbuf.at[block], False)
        other = pair - 2 * (c + 1)
        arrive(other)
        absorb(kbuf.at[other], vbuf.at[other], False)
        return carry

    lax.fori_loop(0, z, level, 0)

    for h in range(heads):
        one = acc[2 * h] / tot[2 * h:2 * h + 1, :]
        two = acc[2 * h + 1] / tot[2 * h + 1:2 * h + 2, :]
        diff = one - lam_ref[h] * two
        scale = lax.rsqrt(jnp.mean(diff * diff, axis=0, keepdims=True) + EPS)
        done = diff * scale * gain_ref[...] * OUT_FACTOR
        rows_ref[:, h * vwidth:(h + 1) * vwidth] = done.T.astype(BF16)

    own = toks // n_tp
    span = heads * vwidth
    column = pl.ds(pl.multiple_of(t * span, span), span)
    sends = []
    for d in range(1, n_tp):
        to = (t + d) % n_tp
        row = pl.ds(pl.multiple_of(to * own, own), own)
        sends.append(
            remote(rows_ref.at[row, :], out_ref.at[:, column], tp_send.at[d], tp_recv.at[d], "tp", to)
        )
    start(sends)
    row = pl.ds(pl.multiple_of(t * own, own), own)
    out_ref[:, column] = rows_ref[row, :]

    @pl.when(z < levels - 1)
    def _():
        for part in copies(me, k_ref, vt_ref, col_send, below):
            part.wait_send()

    @pl.when(x == 0)
    def _():
        for part in copies(me, k_ref, vt_ref, pair_send, pair):
            part.wait_send()

    def drain(c, carry):
        block = me - 2 * (c + 1)

        @pl.when(z < levels - 1)
        def _():
            for part in copies(block, k_ref, vt_ref, col_send, below):
                part.wait_send()

        for part in copies(block, k_ref, vt_ref, pair_send, pair):
            part.wait_send()
        return carry

    lax.fori_loop(0, z, drain, 0)
    for part in sends:
        part.wait()


def greet_all(n_sp, me, t):
    barrier = pltpu.get_barrier_semaphore()

    def hello(d, carry):
        greet("sp", (me + d) % n_sp)
        return carry

    lax.fori_loop(1, n_sp, hello, 0)
    greet("tp", t ^ 1)
    greet("tp", t ^ 2)
    pl.semaphore_wait(barrier, n_sp + 1)


def dispatch_kernel(
    n_sp, pick_ref, rows_ref, buf, out, a_send, a_recv, c_send, c_recv, s_send, s_recv,
):
    me = lax.axis_index("sp")
    t = lax.axis_index("tp")
    sib, cross = t ^ 1, t ^ 2
    greet_all(n_sp, me, t)

    def away(p, d):
        return remote(out.at[p], buf.at[t, me], a_send.at[d], a_recv.at[d], "sp", p)

    def send(d, carry):
        p = (me + d) % n_sp
        out[p] = jnp.dot(pick_ref[p], rows_ref[...], preferred_element_type=F32).astype(BF16)
        away(p, d).start()
        return carry

    lax.fori_loop(1, n_sp, send, 0)
    buf[t, me] = jnp.dot(pick_ref[me], rows_ref[...], preferred_element_type=F32).astype(BF16)

    def over(d):
        s = (me + n_sp - d) % n_sp
        mine = buf.at[t, s]
        theirs = buf.at[cross, s]
        return (
            remote(mine, mine, c_send.at[d], c_recv.at[d], "tp", cross),
            remote(mine, mine, s_send.at[0, d], s_recv.at[0, d], "tp", sib),
            remote(theirs, theirs, s_send.at[1, d], s_recv.at[1, d], "tp", sib),
        )

    first = over(0)
    first[0].start()
    first[1].start()

    def step(d, carry):
        away(me, d).wait_recv()
        now = over(d)
        now[0].start()
        now[1].start()
        before = over(d - 1)
        before[0].wait_recv()
        before[2].start()
        return carry

    lax.fori_loop(1, n_sp, step, 0)
    last = over(n_sp - 1)
    last[0].wait_recv()
    last[2].start()

    def drain(d, carry):
        every = over(d)
        every[0].wait_send()
        every[1].wait()
        every[2].wait()

        @pl.when(d > 0)
        def _():
            away(me, d).wait_send()

        return carry

    lax.fori_loop(0, n_sp, drain, 0)


def combine_kernel(
    n_sp, part, ret, ra, rb, stage, fin, s_send, s_recv, c_send, c_recv, a_send, a_recv,
):
    me = lax.axis_index("sp")
    t = lax.axis_index("tp")
    sib, cross = t ^ 1, t ^ 2
    greet_all(n_sp, me, t)

    def place(d):
        return (me + d) % n_sp

    def side(d, which):
        s = place(d)
        owner = sib if which == 0 else sib ^ 2
        return remote(
            part.at[owner, s], ra.at[which, s], s_send.at[which, d], s_recv.at[which, d], "tp", sib
        )

    def over(d):
        s = place(d)
        return remote(stage.at[s], rb.at[s], c_send.at[d], c_recv.at[d], "tp", cross)

    def back(d):
        s = place(d)
        return remote(fin.at[s], ret.at[me], a_send.at[d], a_recv.at[d], "sp", s)

    def begin(i, carry):
        side((i + 1) % n_sp, 1).start()
        side((i + 1) % n_sp, 0).start()
        return carry

    lax.fori_loop(0, n_sp, begin, 0)

    def middle(i, carry):
        d = (i + 1) % n_sp
        s = place(d)
        side(d, 1).wait_recv()
        stage[s] = (part[cross, s].astype(F32) + ra[1, s].astype(F32)).astype(BF16)
        over(d).start()
        return carry

    lax.fori_loop(0, n_sp, middle, 0)

    def total(d):
        s = place(d)
        side(d, 0).wait_recv()
        over(d).wait_recv()
        return (
            part[t, s].astype(F32) + ra[0, s].astype(F32) + rb[s].astype(F32)
        ).astype(BF16)

    def finish(d, carry):
        fin[place(d)] = total(d)
        back(d).start()
        return carry

    lax.fori_loop(1, n_sp, finish, 0)
    ret[me] = total(0)

    def drain(d, carry):
        side(d, 0).wait_send()
        side(d, 1).wait_send()
        over(d).wait_send()

        @pl.when(d > 0)
        def _():
            back(d).wait()

        return carry

    lax.fori_loop(0, n_sp, drain, 0)


def shards(
    queries, key_vectors, values, head_lambda, head_gain, w_out, residual, ffn_gain,
    route_ids, route_logits, w_gate, w_up, w_down,
):
    toks = queries.shape[0]
    heads = head_lambda.shape[0]
    width = queries.shape[1] // (2 * heads)
    vwidth = values.shape[1] // heads
    n_tp = lax.axis_size("tp")
    n_sp = lax.axis_size("sp")
    model = residual.shape[1]
    own = toks // n_tp
    dma = pltpu.SemaphoreType.DMA

    gates = jax.nn.softmax(route_logits, axis=-1)
    top_count = route_ids.shape[1]
    cap = max(2, 5 * top_count * toks // (4 * n_tp * n_sp))
    slots = -(-cap // 16) * 16
    flat_ids = route_ids.reshape(-1)
    chosen = (flat_ids[:, None] == jnp.arange(n_sp, dtype=jnp.int32)[None, :]).astype(jnp.int32)
    earlier = jnp.cumsum(chosen, axis=0) - chosen
    rank = jnp.sum(earlier * chosen, axis=1)
    slot = (flat_ids * slots + rank).reshape(own, top_count)
    lanes = jnp.arange(n_sp * slots, dtype=jnp.int32)
    hits = [(slot[:, k][:, None] == lanes[None, :]).astype(BF16) for k in range(top_count)]
    pick = sum(hits).T.reshape(n_sp, slots, own)

    whole_weight = lax.all_gather(w_out, "tp", axis=0, tiled=True)

    maps = 2 * heads
    scaled = (queries.astype(F32) * width ** (-0.5)).astype(BF16)
    token_heads = pl.pallas_call(
        functools.partial(attend_kernel, (n_sp, n_tp, heads, width, vwidth, toks)),
        out_shape=jax.ShapeDtypeStruct((own, n_tp * heads * vwidth), BF16),
        in_specs=[SMEM, VMEM, VMEM, VMEM, VMEM],
        out_specs=VMEM,
        scratch_shapes=[
            pltpu.VMEM((n_sp,) + key_vectors.shape, BF16),
            pltpu.VMEM((n_sp,) + values.shape[::-1], BF16),
            pltpu.VMEM((maps, vwidth, toks), F32),
            pltpu.VMEM((maps, toks), F32),
            pltpu.VMEM((maps, toks), F32),
            pltpu.VMEM((toks, heads * vwidth), BF16),
            dma((2, n_sp)), dma((2, n_sp)), dma((2, n_sp)), dma((n_tp,)), dma((n_tp,)),
        ],
        compiler_params=pltpu.CompilerParams(collective_id=0, has_side_effects=True),
        cost_estimate=pl.CostEstimate(flops=2 * 10**10, bytes_accessed=10**7, transcendentals=10**6),
        name="attend",
    )(head_lambda, scaled.T, key_vectors, values.T, head_gain.reshape(vwidth, 1))

    projected = jnp.dot(token_heads, whole_weight, preferred_element_type=F32)
    mixed = (residual.astype(F32) + projected).astype(BF16)
    mixed32 = mixed.astype(F32)
    normed = (
        mixed32 * lax.rsqrt(jnp.mean(mixed32 * mixed32, axis=-1, keepdims=True) + EPS) * ffn_gain
    ).astype(BF16)

    piece = pl.pallas_call(
        functools.partial(dispatch_kernel, n_sp),
        out_shape=jax.ShapeDtypeStruct((n_tp, n_sp, slots, model), BF16),
        in_specs=[VMEM, VMEM],
        out_specs=VMEM,
        scratch_shapes=[
            pltpu.VMEM((n_sp, slots, model), BF16),
            dma((n_sp,)), dma((n_sp,)), dma((n_sp,)), dma((n_sp,)), dma((2, n_sp)), dma((2, n_sp)),
        ],
        compiler_params=pltpu.CompilerParams(collective_id=1, has_side_effects=True),
        name="dispatch",
    )(pick, normed)
    piece = piece.reshape(n_tp * n_sp * slots, model)

    gate_pre = jnp.dot(piece, w_gate[0], preferred_element_type=F32)
    up_pre = jnp.dot(piece, w_up[0], preferred_element_type=F32)
    gate_cut = jnp.minimum(gate_pre, CLAMP)
    up_cut = jnp.clip(up_pre, -CLAMP, CLAMP)
    active = (gate_cut * jax.nn.sigmoid(ALPHA * gate_cut) * (up_cut + 1.0)).astype(BF16)
    part = jnp.dot(active, w_down[0], preferred_element_type=F32).astype(BF16)

    returned = pl.pallas_call(
        functools.partial(combine_kernel, n_sp),
        out_shape=jax.ShapeDtypeStruct((n_sp, slots, model), BF16),
        in_specs=[VMEM],
        out_specs=VMEM,
        scratch_shapes=[
            pltpu.VMEM((2, n_sp, slots, model), BF16),
            pltpu.VMEM((n_sp, slots, model), BF16),
            pltpu.VMEM((n_sp, slots, model), BF16),
            pltpu.VMEM((n_sp, slots, model), BF16),
            dma((2, n_sp)), dma((2, n_sp)), dma((n_sp,)), dma((n_sp,)), dma((n_sp,)), dma((n_sp,)),
        ],
        compiler_params=pltpu.CompilerParams(collective_id=2, has_side_effects=True),
        name="combine",
    )(part.reshape(n_tp, n_sp, slots, model))
    returned = returned.reshape(n_sp * slots, model)
    total = mixed32
    for k in range(top_count):
        total = total + gates[:, k:k + 1] * jnp.dot(hits[k], returned, preferred_element_type=F32)
    return total.astype(BF16)


def solution(mesh):
    in_specs = (
        P("sp", "tp"),
        P("sp", "tp"),
        P("sp", "tp"),
        P("tp"),
        P(),
        P("tp", None),
        P(("sp", "tp"), None),
        P(),
        P(("sp", "tp"), None),
        P(("sp", "tp"), None),
        P("sp", None, "tp"),
        P("sp", None, "tp"),
        P("sp", "tp", None),
    )
    out_specs = P(("sp", "tp"), None)
    return jax.shard_map(shards, mesh=mesh, in_specs=in_specs, out_specs=out_specs, check_vma=False)
```

time: 340 us -> 182 us (0.54); the launches traced: 333 us -> 179 us
  waiting for transfers between devices: 183 us -> 0.7 us
  Pallas kernels: 0 us -> 133 us
  blocking collectives: 42.3 us -> 0 us
  local copies, waits for them, and re-layouts: 36.4 us -> 4.95 us
  starting transfers between devices: 11.3 us -> 0.03 us
  other arithmetic: 11.8 us -> 3.13 us
  matrix products: 30 us -> 22.9 us
  loops' own time: 4.54 us -> 0 us
    pallas_call x0 -> x3, Pallas kernels: none -> 133 us  [the longest x1 60 us: shards(): pl.pallas_call(functools.partial(dispatch_kernel, n_sp), out_shape=jax.Sh...]
    all_gather x3 -> x0, waiting for transfers between devices: 113 us -> none  [the longest x1 42 us: shards(): value_piece = lax.all_gather(values, 'sp', axis=0, tiled=True)]
    reduce_scatter x1 -> x0, waiting for transfers between devices: 42.5 us -> none  [shards(): lax.psum_scatter(jnp.dot(active, w_down[0], preferred_element_type=jnp.fl...]
    all_to_all x1 -> x0, blocking collectives: 42.3 us -> none  [shards(): lax.all_to_all(outgoing, 'sp', split_axis=0, concat_axis=0, tiled=True)]
    all_to_all x2 -> x0, waiting for transfers between devices: 26.1 us -> none  [the longest x1 22.7 us: shards(): lax.all_to_all(reduced, 'sp', split_axis=0, concat_axis=0, tiled=True)]
    all_to_all x2 -> x0, starting transfers between devices: 11 us -> none  [the longest x1 5.5 us: shards(): lax.all_to_all(head_rows, 'tp', split_axis=0, concat_axis=1, tiled=True)]
    reshape x5 -> x1, local copies, waits for them, and re-layouts: 9.02 us -> 0.73 us  [shards(): head_gain.reshape(vwidth, 1)]
    unnamed x31 -> x17, local copies, waits for them, and re-layouts: 11 us -> 3.66 us
  transfers between devices with their start and end apart: 7 -> 1, of which waited for: 6 -> 0; matrix products, arithmetic and copies ran while one was open for 10% -> 4% of each run, Pallas kernels for 0% -> 17%
where the time goes in v1:
time: 182 us; the launch traced here: 179 us
  Pallas kernels  133 us (73%)
  matrix products  22.9 us (13%)
  between operations  13.5 us (7%)
  local copies, waits for them, and re-layouts  4.95 us (3%)
  other arithmetic  3.13 us (2%)
    pallas_call x1, Pallas kernels, shards(): pl.pallas_call(functools.partial(dispatch_kernel, n_sp), out_shape=jax.Sh...  60 us
    pallas_call x1, Pallas kernels, shards(): pl.pallas_call(functools.partial(combine_kernel, n_sp), out_shape=jax.Sha...  42.7 us
    pallas_call x1, Pallas kernels, shards(): pl.pallas_call(functools.partial(attend_kernel, (n_sp, n_tp, heads, width...  30.7 us
    dot_general x1, matrix products, shards(): part = jnp.dot(active, w_down[0], preferred_element_type=F32).astype(BF16)  10.3 us
    dot_general x1, matrix products, shards(): up_pre = jnp.dot(piece, w_up[0], preferred_element_type=F32)  6.58 us
    unnamed x17, local copies, waits for them, and re-layouts  3.66 us
  transfers between devices with their start and end apart: 1, of which 0 were waited for; matrix products, arithmetic and copies ran while one was open for 4% of the time, Pallas kernels for 17%

profile of v1, /device:TPU:13, one launch (start us, length us, event | category | flops | bytes accessed | tf_op | source)
XLA Modules:
  0.0 178.7 jit_solution(14861832997542331166)
XLA Ops:
  6.5 0.0 copy-start
  6.5 0.0 all-gather.2.cloned.1.call-start
  6.6 0.7 all-gather.2.cloned.1.call-update
  7.3 0.8 copy.32
  8.1 0.1 eq.78
  8.2 0.6 reduce-window.6
  8.8 0.2 slice_reduce_fusion
  9.1 0.1 add_bitcast_fusion
  9.2 0.1 reduce_sum.31
  9.3 0.1 copy.33
  9.4 1.1 copy.29
  10.5 1.7 copy.30
  12.2 0.0 copy-done.6
  12.2 0.7 copy.31.gain_ref
  13.0 0.0 copy-done.3
  13.0 0.0 copy-done.5
  13.1 0.7 fusion.15.pick_ref
  13.8 0.7 fusion.14.qt_ref
  14.5 30.7 %attend.1 = bf16[96,1024]{1,0:T(8,128)(2,1)} custom-call(f32[2]{0:T(128)} %lam_ref.1, bf16[256,384]{1,0:T(8,128)(2,1)} %fusion.14.qt_ref, bf16[384,256]{1,0:T(8,128)(2,1)} %k_ref.1, bf16[256,384]{1,0:T(8,128)(2,1)} %bitcast.45, f32[128,1]{1,0:T(8,128)} %copy.31.gain_ref), custom_call_target="tpu_custom_call" | custom-call | flops 20000000000 | bytes 10000000 | tf_op jit(solution)/shard_map/attend/pallas_call | solution.py:378
  45.2 0.0 copy-start.4
  45.3 0.0 all-gather.2.cloned.1.call-done
  45.3 0.0 copy-done.2
  45.3 3.3 %multiply_reduce_fusion = (f32[96]{0:T(128)S(1)}, f32[96,2048]{1,0:T(8,128)S(1)}) fusion(bf16[96,1024]{1,0:T(8,128)(2,1)} %attend.1, bf16[1024,2048]{1,0:T(8,128)(2,1)} %all-gather.2.cloned.1.call-done, bf16[96,2048]{1,0:T(8,128)(2,1)S(1)} %copy-done.2), kind=kOutput, calls=%fused_computation.16 | convolution fusion | flops 403832736 | bytes 5570944 | tf_op jit(solution)/shard_map/dot_general | solution.py:397
  48.6 0.0 copy-done.4
  48.6 0.9 multiply_convert_fusion.1.rows_ref
  49.5 60.0 %dispatch.1 = bf16[4,8,32,2048]{3,2,1,0:T(8,128)(2,1)} custom-call(bf16[8,32,96]{2,1,0:T(8,128)(2,1)} %fusion.15.pick_ref, bf16[96,2048]{1,0:T(8,128)(2,1)} %multiply_convert_fusion.1.rows_ref), custom_call_target="tpu_custom_call" | custom-call | tf_op jit(solution)/shard_map/dispatch/pallas_call | solution.py:404
  109.5 6.6 %fusion.6 = f32[1024,512]{1,0:T(8,128)} fusion(bf16[1024,2048]{1,0:T(8,128)(2,1)} %bitcast.43, bf16[1,2048,512]{2,1,0:T(8,128)(2,1)} %param.24), kind=kOutput, calls=%fused_computation.10 | convolution fusion | flops 2147483648 | bytes 8388608 | tf_op jit(solution)/shard_map/dot_general | solution.py:419
  116.1 10.3 %convolution_convert_fusion = bf16[1024,2048]{1,0:T(8,128)(2,1)} fusion(bf16[1,512,2048]{2,1,0:T(8,128)(2,1)S(1)} %copy-done, f32[1024,512]{1,0:T(8,128)} %fusion.6, bf16[1024,2048]{1,0:T(8,128)(2,1)} %bitcast.44, bf16[1,2048,512]{2,1,0:T(8,128)(2,1)} %param.23), kind=kOutput, calls=%fused_computation | convolution fusion | flops 4302307328 | bytes 14680064 | tf_op jit(solution)/shard_map/dot_general | solution.py:423
  126.4 42.7 %combine.1 = bf16[8,32,2048]{2,1,0:T(8,128)(2,1)} custom-call(bf16[4,8,32,2048]{3,2,1,0:T(8,128)(2,1)} %bitcast.42), custom_call_target="tpu_custom_call" | custom-call | tf_op jit(solution)/shard_map/combine/pallas_call | solution.py:425
  169.1 0.0 copy-start.1
  169.1 1.7 fusion.1
  170.7 1.1 fusion.4
  (19 shorter events, 0.2 us)
Async XLA Ops:
  6.5 109.6 %copy-start = (bf16[1,512,2048]{2,1,0:T(8,128)(2,1)S(1)}, bf16[1,512,2048]{2,1,0:T(8,128)(2,1)}, u32[]{:S(2)}) copy-start(bf16[1,512,2048]{2,1,0:T(8,128)(2,1)} %param.25) | copy-start | bytes 6291460
  6.5 6.5 %copy-start.5 = (s32[96,2]{0,1:T(2,128)S(1)}, s32[96,2]{0,1:T(2,128)}, u32[]{:S(2)}) copy-start(s32[96,2]{0,1:T(2,128)} %param.21) | copy-start | bytes 2308
  6.5 5.7 %copy-start.6 = (f32[128]{0:T(128)S(1)}, f32[128]{0:T(128)}, u32[]{:S(2)}) copy-start(f32[128]{0:T(128)} %param.17) | copy-start | bytes 1540
  6.5 6.4 %copy-start.3 = (f32[96,2]{0,1:T(2,128)S(1)}, f32[96,2]{0,1:T(2,128)}, u32[]{:S(2)}) copy-start(f32[96,2]{0,1:T(2,128)} %param.22) | copy-start | bytes 2308
  6.5 38.7 %all-gather.2.cloned.1.call-start = ((), (), s32[]{:S(2)}) async-start(), calls=%async_computation | async-start | bytes 5242880 | tf_op jit(solution)/shard_map/all_gather | solution.py:374
  14.5 30.8 %copy-start.2 = (bf16[96,2048]{1,0:T(8,128)(2,1)S(1)}, bf16[96,2048]{1,0:T(8,128)(2,1)}, u32[]{:S(2)}) copy-start(bf16[96,2048]{1,0:T(8,128)(2,1)} %param.19) | copy-start | bytes 1179652
  45.2 3.3 %copy-start.4 = (f32[2048]{0:T(1024)S(1)}, f32[2048]{0:T(1024)}, u32[]{:S(2)}) copy-start(f32[2048]{0:T(1024)} %param.20) | copy-start | bytes 24580
  169.1 1.7 copy-start.1
Sparse Core Ops, SparseCore 0:
  8.9 35.5 all-gather.1

commit v2 on v1

--- a/solution.py
+++ b/solution.py
@@ -194,149 +194,159 @@
         part.wait()
 
 
-def greet_all(n_sp, me, t):
-    barrier = pltpu.get_barrier_semaphore()
-
-    def hello(d, carry):
-        greet("sp", (me + d) % n_sp)
-        return carry
-
-    lax.fori_loop(1, n_sp, hello, 0)
-    greet("tp", t ^ 1)
-    greet("tp", t ^ 2)
-    pl.semaphore_wait(barrier, n_sp + 1)
-
-
-def dispatch_kernel(
-    n_sp, pick_ref, rows_ref, buf, out, a_send, a_recv, c_send, c_recv, s_send, s_recv,
+def experts_kernel(
+    n_sp, n_tp, pick_ref, rows_ref, gate_hbm, up_hbm, down_hbm, ret,
+    out, buf, part, ra, rb, wg, wu, wd, w_sem,
+    a_send, a_recv, c_send, c_recv, s_send, s_recv,
+    p_send, p_recv, o_send, o_recv, b_send, b_recv,
 ):
     me = lax.axis_index("sp")
     t = lax.axis_index("tp")
     sib, cross = t ^ 1, t ^ 2
-    greet_all(n_sp, me, t)
-
-    def away(p, d):
-        return remote(out.at[p], buf.at[t, me], a_send.at[d], a_recv.at[d], "sp", p)
-
-    def send(d, carry):
-        p = (me + d) % n_sp
-        out[p] = jnp.dot(pick_ref[p], rows_ref[...], preferred_element_type=F32).astype(BF16)
-        away(p, d).start()
-        return carry
-
-    lax.fori_loop(1, n_sp, send, 0)
-    buf[t, me] = jnp.dot(pick_ref[me], rows_ref[...], preferred_element_type=F32).astype(BF16)
-
-    def over(d):
-        s = (me + n_sp - d) % n_sp
-        mine = buf.at[t, s]
-        theirs = buf.at[cross, s]
-        return (
-            remote(mine, mine, c_send.at[d], c_recv.at[d], "tp", cross),
-            remote(mine, mine, s_send.at[0, d], s_recv.at[0, d], "tp", sib),
-            remote(theirs, theirs, s_send.at[1, d], s_recv.at[1, d], "tp", sib),
-        )
-
-    first = over(0)
-    first[0].start()
-    first[1].start()
-
-    def step(d, carry):
-        away(me, d).wait_recv()
-        now = over(d)
-        now[0].start()
-        now[1].start()
-        before = over(d - 1)
-        before[0].wait_recv()
-        before[2].start()
-        return carry
-
-    lax.fori_loop(1, n_sp, step, 0)
-    last = over(n_sp - 1)
-    last[0].wait_recv()
-    last[2].start()
-
-    def drain(d, carry):
-        every = over(d)
-        every[0].wait_send()
-        every[1].wait()
-        every[2].wait()
-
-        @pl.when(d > 0)
-        def _():
-            away(me, d).wait_send()
-
-        return carry
-
-    lax.fori_loop(0, n_sp, drain, 0)
-
-
-def combine_kernel(
-    n_sp, part, ret, ra, rb, stage, fin, s_send, s_recv, c_send, c_recv, a_send, a_recv,
-):
-    me = lax.axis_index("sp")
-    t = lax.axis_index("tp")
-    sib, cross = t ^ 1, t ^ 2
-    greet_all(n_sp, me, t)
-
-    def place(d):
-        return (me + d) % n_sp
+    slots, model = out.shape[1:]
+    chunks = n_sp // 2
+    loads = [
+        pltpu.make_async_copy(src.at[0], dst, w_sem.at[i])
+        for i, (src, dst) in enumerate(((gate_hbm, wg), (up_hbm, wu), (down_hbm, wd)))
+    ]
+    for load in loads:
+        load.start()
+
+    def hello(d, carry):
+        greet("sp", me ^ d)
+        return carry
+
+    lax.fori_loop(1, n_sp, hello, 0)
+    greet("tp", sib)
+    greet("tp", cross)
+    pl.semaphore_wait(pltpu.get_barrier_semaphore(), n_sp + 1)
+
+    def chosen(p):
+        return jnp.dot(pick_ref[p], rows_ref[...], preferred_element_type=F32).astype(BF16)
+
+    def away(d):
+        return remote(out.at[d], buf.at[d, t], a_send.at[d], a_recv.at[d], "sp", me ^ d)
+
+    def across(d):
+        mine = buf.at[d, t]
+        return remote(mine, mine, c_send.at[d], c_recv.at[d], "tp", cross)
+
+    def beside(d, which):
+        block = buf.at[d, t if which == 0 else cross]
+        return remote(block, block, s_send.at[which, d], s_recv.at[which, d], "tp", sib)
 
     def side(d, which):
-        s = place(d)
         owner = sib if which == 0 else sib ^ 2
         return remote(
-            part.at[owner, s], ra.at[which, s], s_send.at[which, d], s_recv.at[which, d], "tp", sib
+            part.at[d, owner], ra.at[which, d], p_send.at[which, d], p_recv.at[which, d], "tp", sib
         )
 
     def over(d):
-        s = place(d)
-        return remote(stage.at[s], rb.at[s], c_send.at[d], c_recv.at[d], "tp", cross)
+        return remote(part.at[d, cross], rb.at[d], o_send.at[d], o_recv.at[d], "tp", cross)
 
     def back(d):
-        s = place(d)
-        return remote(fin.at[s], ret.at[me], a_send.at[d], a_recv.at[d], "sp", s)
-
-    def begin(i, carry):
-        side((i + 1) % n_sp, 1).start()
-        side((i + 1) % n_sp, 0).start()
-        return carry
-
-    lax.fori_loop(0, n_sp, begin, 0)
-
-    def middle(i, carry):
-        d = (i + 1) % n_sp
-        s = place(d)
+        return remote(part.at[d, t], ret.at[me], b_send.at[d], b_recv.at[d], "sp", me ^ d)
+
+    buf[0, t] = chosen(me)
+
+    def send(d, carry):
+        out[d] = chosen(me ^ d)
+        away(d).start()
+        return carry
+
+    lax.fori_loop(1, n_sp, send, 0)
+    for load in loads:
+        load.wait()
+
+    def forward(d):
+        @pl.when(d > 0)
+        def _():
+            away(d).wait_recv()
+
+        across(d).start()
+        beside(d, 0).start()
+
+    def relay(d):
+        across(d).wait_recv()
+        beside(d, 1).start()
+
+    def multiply(c):
+        for d in (2 * c, 2 * c + 1):
+            beside(d, 0).wait_recv()
+            beside(d, 1).wait_recv()
+        rows = buf[pl.ds(2 * c, 2)].reshape(2 * n_tp * slots, model)
+        gate = jnp.minimum(jnp.dot(rows, wg[...], preferred_element_type=F32), CLAMP)
+        up = jnp.clip(jnp.dot(rows, wu[...], preferred_element_type=F32), -CLAMP, CLAMP)
+        active = (gate * jax.nn.sigmoid(ALPHA * gate) * (up + 1.0)).astype(BF16)
+        step = 512 if model % 512 == 0 else model
+        for first in range(0, model, step):
+            piece = jnp.dot(active, wd[:, first:first + step], preferred_element_type=F32)
+            part[pl.ds(2 * c, 2), :, :, first:first + step] = piece.astype(BF16).reshape(
+                2, n_tp, slots, step
+            )
+        for d in (2 * c, 2 * c + 1):
+            side(d, 1).start()
+        for d in (2 * c, 2 * c + 1):
+            side(d, 0).start()
+
+    def middle(d):
         side(d, 1).wait_recv()
-        stage[s] = (part[cross, s].astype(F32) + ra[1, s].astype(F32)).astype(BF16)
+        part[d, cross] = (part[d, cross].astype(F32) + ra[1, d].astype(F32)).astype(BF16)
         over(d).start()
-        return carry
-
-    lax.fori_loop(0, n_sp, middle, 0)
-
-    def total(d):
-        s = place(d)
+
+    def finish(d):
         side(d, 0).wait_recv()
         over(d).wait_recv()
-        return (
-            part[t, s].astype(F32) + ra[0, s].astype(F32) + rb[s].astype(F32)
+        done = (
+            part[d, t].astype(F32) + ra[0, d].astype(F32) + rb[d].astype(F32)
         ).astype(BF16)
 
-    def finish(d, carry):
-        fin[place(d)] = total(d)
-        back(d).start()
-        return carry
-
-    lax.fori_loop(1, n_sp, finish, 0)
-    ret[me] = total(0)
+        @pl.when(d > 0)
+        def _():
+            part[d, t] = done
+            back(d).start()
+
+        @pl.when(d == 0)
+        def _():
+            ret[me] = done
+
+    def both(act, c):
+        act(2 * c)
+        act(2 * c + 1)
+
+    def advance(i, carry):
+        @pl.when(i < chunks)
+        def _():
+            both(forward, i)
+
+        @pl.when((i >= 1) & (i <= chunks))
+        def _():
+            both(relay, i - 1)
+            multiply(i - 1)
+
+        @pl.when(i >= 2)
+        def _():
+            both(finish, i - 2)
+
+        @pl.when((i >= 1) & (i <= chunks))
+        def _():
+            both(middle, i - 1)
+
+        return carry
+
+    lax.fori_loop(0, chunks + 2, advance, 0)
 
     def drain(d, carry):
+        across(d).wait_send()
+        beside(d, 0).wait_send()
+        beside(d, 1).wait_send()
         side(d, 0).wait_send()
         side(d, 1).wait_send()
         over(d).wait_send()
 
         @pl.when(d > 0)
         def _():
+            away(d).wait_send()
             back(d).wait()
 
         return carry
@@ -401,42 +411,32 @@
         mixed32 * lax.rsqrt(jnp.mean(mixed32 * mixed32, axis=-1, keepdims=True) + EPS) * ffn_gain
     ).astype(BF16)
 
-    piece = pl.pallas_call(
-        functools.partial(dispatch_kernel, n_sp),
-        out_shape=jax.ShapeDtypeStruct((n_tp, n_sp, slots, model), BF16),
-        in_specs=[VMEM, VMEM],
+    block = (n_sp, slots, model)
+    ff = w_gate.shape[2]
+    hbm = pl.BlockSpec(memory_space=pl.ANY)
+    lone, twin = dma((n_sp,)), dma((2, n_sp))
+    returned = pl.pallas_call(
+        functools.partial(experts_kernel, n_sp, n_tp),
+        out_shape=jax.ShapeDtypeStruct(block, BF16),
+        in_specs=[VMEM, VMEM, hbm, hbm, hbm],
         out_specs=VMEM,
         scratch_shapes=[
-            pltpu.VMEM((n_sp, slots, model), BF16),
-            dma((n_sp,)), dma((n_sp,)), dma((n_sp,)), dma((n_sp,)), dma((2, n_sp)), dma((2, n_sp)),
+            pltpu.VMEM(block, BF16),
+            pltpu.VMEM((n_sp, n_tp, slots, model), BF16),
+            pltpu.VMEM((n_sp, n_tp, slots, model), BF16),
+            pltpu.VMEM((2,) + block, BF16),
+            pltpu.VMEM(block, BF16),
+            pltpu.VMEM((model, ff), BF16),
+            pltpu.VMEM((model, ff), BF16),
+            pltpu.VMEM((ff, model), BF16),
+            dma((3,)),
+            lone, lone, lone, lone, twin, twin, twin, twin, lone, lone, lone, lone,
         ],
-        compiler_params=pltpu.CompilerParams(collective_id=1, has_side_effects=True),
-        name="dispatch",
-    )(pick, normed)
-    piece = piece.reshape(n_tp * n_sp * slots, model)
-
-    gate_pre = jnp.dot(piece, w_gate[0], preferred_element_type=F32)
-    up_pre = jnp.dot(piece, w_up[0], preferred_element_type=F32)
-    gate_cut = jnp.minimum(gate_pre, CLAMP)
-    up_cut = jnp.clip(up_pre, -CLAMP, CLAMP)
-    active = (gate_cut * jax.nn.sigmoid(ALPHA * gate_cut) * (up_cut + 1.0)).astype(BF16)
-    part = jnp.dot(active, w_down[0], preferred_element_type=F32).astype(BF16)
-
-    returned = pl.pallas_call(
-        functools.partial(combine_kernel, n_sp),
-        out_shape=jax.ShapeDtypeStruct((n_sp, slots, model), BF16),
-        in_specs=[VMEM],
-        out_specs=VMEM,
-        scratch_shapes=[
-            pltpu.VMEM((2, n_sp, slots, model), BF16),
-            pltpu.VMEM((n_sp, slots, model), BF16),
-            pltpu.VMEM((n_sp, slots, model), BF16),
-            pltpu.VMEM((n_sp, slots, model), BF16),
-            dma((2, n_sp)), dma((2, n_sp)), dma((n_sp,)), dma((n_sp,)), dma((n_sp,)), dma((n_sp,)),
-        ],
-        compiler_params=pltpu.CompilerParams(collective_id=2, has_side_effects=True),
-        name="combine",
-    )(part.reshape(n_tp, n_sp, slots, model))
+        compiler_params=pltpu.CompilerParams(
+            collective_id=1, has_side_effects=True, vmem_limit_bytes=67043328
+        ),
+        name="experts",
+    )(pick, normed, w_gate, w_up, w_down)
     returned = returned.reshape(n_sp * slots, model)
     total = mixed32
     for k in range(top_count):

time: 182 us -> 160 us (0.88); the launches traced: 179 us -> 160 us
  matrix products: 22.9 us -> 7.39 us
  Pallas kernels: 133 us -> 125 us
  other arithmetic: 3.13 us -> 5.86 us
  local copies, waits for them, and re-layouts: 4.95 us -> 7.06 us
    dot_general x2 -> x0, matrix products: 16.9 us -> none  [the longest x1 10.3 us: shards(): part = jnp.dot(active, w_down[0], preferred_element_type=F32).astype(BF16)]
    pallas_call x2 -> x1, Pallas kernels: 103 us -> 94.7 us  [shards(): pl.pallas_call(functools.partial(experts_kernel, n_sp, n_tp), out_shape=j...]
    unnamed x17 -> x13, local copies, waits for them, and re-layouts: 3.66 us -> 4.54 us
  transfers between devices with their start and end apart: 1 -> 1, of which waited for: 0 -> 0; matrix products, arithmetic and copies ran while one was open for 4% -> 7% of each run, Pallas kernels for 17% -> 19%
where the time goes in v2:
time: 160 us
  Pallas kernels  125 us (78%)
  between operations  13.5 us (8%)
  matrix products  7.39 us (5%)
  local copies, waits for them, and re-layouts  7.06 us (4%)
  other arithmetic  5.86 us (4%)
    pallas_call x1, Pallas kernels, shards(): pl.pallas_call(functools.partial(experts_kernel, n_sp, n_tp), out_shape=j...  94.7 us
    pallas_call x1, Pallas kernels, shards(): pl.pallas_call(functools.partial(attend_kernel, (n_sp, n_tp, heads, width...  30.7 us
    unnamed x13, local copies, waits for them, and re-layouts  4.54 us
    dot_general x2, matrix products, shards(): jnp.dot(hits[k], returned, preferred_element_type=F32)  4.13 us
    dot_general x1, matrix products, shards(): projected = jnp.dot(token_heads, whole_weight, preferred_element_type=F32)  3.26 us
  transfers between devices with their start and end apart: 1, of which 0 were waited for; matrix products, arithmetic and copies ran while one was open for 7% of the time, Pallas kernels for 19%

profile of v2, /device:TPU:13, one launch (start us, length us, event | category | flops | bytes accessed | tf_op | source)
XLA Modules:
  0.0 159.9 jit_solution(9088861070340074303)
XLA Ops:
  6.5 0.0 all-gather.2.cloned.1.call-start
  6.5 0.7 all-gather.2.cloned.1.call-update
  7.3 1.1 copy.29
  8.3 1.7 %copy.30 = bf16[384,256]{0,1:T(8,128)(2,1)} copy(bf16[384,256]{1,0:T(8,128)(2,1)} %param.15) | data formatting | bytes 393216 | tf_op args[2]
  10.1 1.4 copy.31.gain_ref
  11.5 0.8 copy.32
  12.2 0.1 eq.78
  12.4 0.6 reduce-window.6
  13.0 0.2 slice_reduce_fusion
  13.2 0.1 add_bitcast_fusion
  13.4 0.1 reduce_sum.31
  13.5 0.1 copy.33
  13.6 0.7 reduce_max.9
  14.3 0.7 fusion.12
  15.0 0.7 multiply_add_fusion.1
  15.7 0.7 fusion.11
  16.4 0.6 slice_bitcast_fusion
  17.0 0.7 fusion.6.pick_ref
  17.7 0.7 fusion.5.qt_ref
  18.4 0.0 copy-done.3
  18.4 0.0 copy-done.4
  18.4 30.7 %attend.1 = bf16[96,1024]{1,0:T(8,128)(2,1)} custom-call(f32[2]{0:T(128)} %lam_ref.1, bf16[256,384]{1,0:T(8,128)(2,1)} %fusion.5.qt_ref, bf16[384,256]{1,0:T(8,128)(2,1)} %k_ref.1, bf16[256,384]{1,0:T(8,128)(2,1)} %bitcast.25, f32[128,1]{1,0:T(8,128)} %copy.31.gain_ref), custom_call_target="tpu_custom_call" | custom-call | flops 20000000000 | bytes 10000000 | tf_op jit(solution)/shard_map/attend/pallas_call | solution.py:388
  49.1 0.0 copy-start.2
  49.1 0.0 all-gather.2.cloned.1.call-done
  49.1 0.0 copy-done.1
  49.2 3.3 %multiply_reduce_fusion = (f32[96]{0:T(128)S(1)}, f32[96,2048]{1,0:T(8,128)S(1)}) fusion(bf16[96,1024]{1,0:T(8,128)(2,1)} %attend.1, bf16[1024,2048]{1,0:T(8,128)(2,1)} %all-gather.2.cloned.1.call-done, bf16[96,2048]{1,0:T(8,128)(2,1)S(1)} %copy-done.1), kind=kOutput, calls=%fused_computation.9 | convolution fusion | flops 403832736 | bytes 5570944 | tf_op jit(solution)/shard_map/dot_general | solution.py:407
  52.4 0.0 copy-start
  52.4 0.9 copy-done
  53.4 0.9 multiply_convert_fusion.rows_ref
  54.2 94.7 %experts.1 = bf16[8,32,2048]{2,1,0:T(8,128)(2,1)} custom-call(bf16[8,32,96]{2,1,0:T(8,128)(2,1)} %fusion.6.pick_ref, bf16[96,2048]{1,0:T(8,128)(2,1)} %multiply_convert_fusion.rows_ref, bf16[1,2048,512]{2,1,0:T(8,128)(2,1)} %gate_hbm.1, bf16[1,2048,512]{2,1,0:T(8,128)(2,1)} %up_hbm.1, bf16[1,512,2048]{2,1,0:T(8,128)(2,1)} %down_hbm.1), custom_call_target="tpu_custom_call" | custom-call | tf_op jit(solution)/shard_map/experts/pallas_call | solution.py:418
  148.9 1.8 %fusion.1 = f32[96,2048]{1,0:T(8,128)S(1)} fusion(f32[96,2048]{1,0:T(8,128)} %copy-done, bf16[256,2048]{1,0:T(8,128)(2,1)} %bitcast.23, f32[96]{0:T(128)} %get-tuple-element.6, s32[96]{0:T(128)} %copy-done.3), kind=kOutput, calls=%fused_computation.4 | convolution fusion | flops 101081088 | bytes 2622208 | tf_op jit(solution)/shard_map/dot_general | solution.py:443
  150.7 2.3 %fusion.4 = bf16[96,2048]{1,0:T(8,128)(2,1)} fusion(f32[96,2048]{1,0:T(8,128)S(1)} %fusion.1, bf16[256,2048]{1,0:T(8,128)(2,1)} %bitcast.24, f32[96]{0:T(128)} %get-tuple-element.5, s32[96]{0:T(128)} %copy-done.4), kind=kOutput, calls=%fused_computation.7 | convolution fusion | flops 101277696 | bytes 2228992 | tf_op jit(solution)/shard_map/dot_general | solution.py:443
  (12 shorter events, 0.1 us)
Async XLA Ops:
  6.5 42.6 %all-gather.2.cloned.1.call-start = ((), (), s32[]{:S(2)}) async-start(), calls=%async_computation | async-start | bytes 5242880 | tf_op jit(solution)/shard_map/all_gather | solution.py:384
  15.7 2.7 %copy-start.3 = (s32[96]{0:T(128)}, s32[96]{0:T(128)S(1)}, u32[]{:S(2)}) copy-start(s32[96]{0:T(128)S(1)} %get-tuple-element.7) | copy-start | bytes 1156
  15.7 2.7 %copy-start.4 = (s32[96]{0:T(128)}, s32[96]{0:T(128)S(1)}, u32[]{:S(2)}) copy-start(s32[96]{0:T(128)S(1)} %get-tuple-element.8) | copy-start | bytes 1156
  18.4 30.7 %copy-start.1 = (bf16[96,2048]{1,0:T(8,128)(2,1)S(1)}, bf16[96,2048]{1,0:T(8,128)(2,1)}, u32[]{:S(2)}) copy-start(bf16[96,2048]{1,0:T(8,128)(2,1)} %param.19) | copy-start | bytes 1179652
  49.1 4.2 %copy-start.2 = (f32[2048]{0:T(1024)S(1)}, f32[2048]{0:T(1024)}, u32[]{:S(2)}) copy-start(f32[2048]{0:T(1024)} %param.20) | copy-start | bytes 24580
  52.4 0.9 copy-start
Sparse Core Ops, SparseCore 0:
  8.9 35.0 all-gather.1
